TPU v7x, 128 devices: a whole 4x4x4 slice. The times are simulated.
128 devices in a mesh: sp: 16 (over z, y), tp: 8 (over x, core).
Axes of the slice: x: 4, y: 4, z: 4, core: 2. Of those that a mesh axis runs over, the one named last changes fastest.
Arguments:
- inputs: bfloat16 [8192, 4096], P(('sp', 'tp')), may hold values from -42 to 42
- a_query_w: bfloat16 [4096, 2048], P(None, 'tp'), may hold values from -0.12570312 to 0.12570312
- a_key_w: bfloat16 [4096, 2048], P(None, 'tp'), may hold values from -0.12570312 to 0.12570312
- a_value_w: bfloat16 [4096, 2048], P(None, 'tp'), may hold values from -0.09375 to 0.09375
- b_query_w: bfloat16 [4096, 2048], P(None, 'tp'), may hold values from -0.12570312 to 0.12570312
- b_key_w: bfloat16 [4096, 512], P(None, 'tp'), may hold values from -0.12570312 to 0.12570312
- b_value_w: bfloat16 [4096, 512], P(None, 'tp'), may hold values from -0.09375 to 0.09375
- head_lambda: float32 [16], P('tp'), may hold values from 0.3 to 0.8
- head_gain: float32 [128], replicated, may hold values from 0.1 to 1.9
- sink_logit: float32 [32], P('tp'), may hold values from 2 to 7
- a_out_w: bfloat16 [2048, 4096], P('tp'), may hold values from -0.125 to 0.125
- b_out_w: bfloat16 [2048, 4096], P('tp'), may hold values from -0.625 to 0.625
Outputs:
- mixed: bfloat16 [8192, 4096], P(('sp', 'tp'))
All inputs are finite; a program needn't handle non-finite values.
Results may differ from a plain program's by a relative error of at most 0.015.
Values may be sent and summed in bfloat16 or wider, within the bound.
A program may use at most 128 MiB of HBM per device.

v0:
```python
import math
import jax
import jax.numpy as jnp
from jax import lax
from jax.sharding import PartitionSpec as P

HEAD_DIM = 64
VALUE_DIM = 128
WINDOW = 128
norm_eps = 0.0001
head_scale = 0.8
mask_fill = -1e30


def from_behind(value, axis, by):
    size = lax.axis_size(axis)
    pairs = [(i, i + by) for i in range(size) if 0 <= i + by < size]
    return lax.ppermute(value, axis, pairs)


def side_by_side(arrays, axis, dim, along):
    widths = [a.shape[along] for a in arrays]
    both = jnp.concatenate(arrays, axis=along)
    whole = lax.all_gather(both, axis, axis=dim, tiled=True)
    return tuple(jnp.split(whole, [sum(widths[:k]) for k in range(1, len(widths))], axis=along))


def key_span(row_count):
    span_rows = math.gcd(row_count, 1024)
    return span_rows


def attend_block(carried, queries, query_pos, block_keys, block_values, key_pos):
    running, totals, numerator = carried
    scores = jnp.einsum(
        "qhmd,khmd->hmqk", queries, block_keys, preferred_element_type=jnp.float32
    ) * HEAD_DIM ** (-0.5)
    allowed = query_pos[:, None] >= key_pos[None, :]
    scores = jnp.where(allowed, scores, mask_fill)
    updated = jnp.maximum(running, jnp.max(scores, axis=-1))
    weights = jnp.where(allowed, jnp.exp(scores - updated[..., None]), 0.0)
    shrink = jnp.exp(running - updated)
    totals = totals * shrink + jnp.sum(weights, axis=-1)
    numerator = numerator * shrink[..., None] + jnp.einsum(
        "hmqk,khe->hmqe",
        weights.astype(jnp.bfloat16),
        block_values,
        preferred_element_type=jnp.float32,
    )
    return (updated, totals, numerator)


def advance(states, groups, key_rows, value_rows):
    row_count = key_rows.shape[0]
    span_rows = key_span(row_count)
    local_heads = value_rows.shape[1] // VALUE_DIM
    key_rows = key_rows.reshape(row_count, local_heads, 2, HEAD_DIM)
    value_rows = value_rows.reshape(row_count, local_heads, VALUE_DIM)

    def one_span(span_index, current):
        span_start = span_index * span_rows
        block_keys = lax.dynamic_slice_in_dim(key_rows, span_start, span_rows, 0)
        block_values = lax.dynamic_slice_in_dim(value_rows, span_start, span_rows, 0)
        key_pos = span_start + jnp.arange(span_rows, dtype=jnp.int32)
        results = []
        for query_group, carried in zip(groups, current):
            queries, query_pos = query_group

            def compute(given_state, queries=queries, query_pos=query_pos):
                return attend_block(
                    given_state, queries, query_pos, block_keys, block_values, key_pos
                )

            def unchanged(given_state):
                return given_state

            results.append(lax.cond(key_pos[0] <= query_pos[-1], compute, unchanged, carried))
        return tuple(results)

    return lax.fori_loop(0, row_count // span_rows, one_span, states)


def finish_heads(carried, head_lambda, head_gain):
    running, totals, numerator = carried
    means = numerator / totals[..., None]
    difference = means[:, 0] - head_lambda[:, None, None] * means[:, 1]
    mean_square = jnp.mean(difference * difference, axis=-1, keepdims=True)
    return (difference * lax.rsqrt(mean_square + norm_eps) * head_gain * head_scale).astype(
        jnp.bfloat16
    )


def shards(
    inputs,
    a_query_w,
    a_key_w,
    a_value_w,
    b_query_w,
    b_key_w,
    b_value_w,
    head_lambda,
    head_gain,
    sink_logit,
    a_out_w,
    b_out_w,
):
    matrices = (a_query_w, a_key_w, a_value_w, b_query_w, b_key_w, b_value_w)

    def project(shard_piece):
        return jnp.concatenate(
            [
                jnp.dot(shard_piece, matrix, preferred_element_type=jnp.float32).astype(
                    jnp.bfloat16
                )
                for matrix in matrices
            ],
            axis=1,
        )

    projected = project(lax.all_gather(inputs, "tp", axis=0, tiled=True))
    seg_rows = projected.shape[0]
    column_edges = [0]
    for matrix in matrices:
        column_edges.append(column_edges[-1] + matrix.shape[1])
    a_query = projected[:, column_edges[0] : column_edges[1]]
    a_key = projected[:, column_edges[1] : column_edges[2]]
    a_value = projected[:, column_edges[2] : column_edges[3]]
    b_query = projected[:, column_edges[3] : column_edges[4]]
    b_pair = projected[:, column_edges[4] : column_edges[6]]
    local_heads = head_lambda.shape[0]
    offset = lax.axis_index("sp") * seg_rows
    positions = offset + jnp.arange(seg_rows, dtype=jnp.int32)
    query_heads = a_query.reshape(seg_rows, local_heads, 2, HEAD_DIM)
    groups = ((query_heads, positions),)
    initial = tuple(
        (
            (
                jnp.full((local_heads, 2, group_queries.shape[0]), mask_fill, jnp.float32),
                jnp.zeros((local_heads, 2, group_queries.shape[0]), jnp.float32),
                jnp.zeros((local_heads, 2, group_queries.shape[0], VALUE_DIM), jnp.float32),
            )
            for group_queries, group_pos in groups
        )
    )
    earlier = from_behind(b_pair[seg_rows - WINDOW :], "sp", 1)
    shard_piece = side_by_side((a_key, a_value), "sp", 0, 1)
    states = advance(initial, groups, shard_piece[0], shard_piece[1])
    finished = [finish_heads(carried, head_lambda, head_gain) for carried in states]
    a_heads = finished[0]
    kv_heads = b_pair.shape[1] // (2 * HEAD_DIM)
    group_size = b_query.shape[1] // HEAD_DIM // kv_heads
    extended = jnp.concatenate([earlier, b_pair], axis=0)
    near_keys = extended[:, : kv_heads * HEAD_DIM].reshape(WINDOW + seg_rows, kv_heads, HEAD_DIM)
    near_values = extended[:, kv_heads * HEAD_DIM :].reshape(WINDOW + seg_rows, kv_heads, HEAD_DIM)
    window_queries = b_query.reshape(seg_rows, kv_heads, group_size, HEAD_DIM)
    sink_term = sink_logit.reshape(kv_heads, group_size)[:, :, None]
    query_span = math.gcd(seg_rows, 512)
    scores = jnp.einsum(
        "qhgd,khd->hgqk", window_queries, near_keys, preferred_element_type=jnp.float32
    ) * HEAD_DIM ** (-0.5)
    query_pos = offset + 0 + jnp.arange(query_span, dtype=jnp.int32)
    near_pos = offset + 0 - WINDOW + jnp.arange(query_span + WINDOW, dtype=jnp.int32)
    distance = query_pos[:, None] - near_pos[None, :]
    allowed = (distance >= 0) & (distance < WINDOW) & (near_pos[None, :] >= 0)
    scores = jnp.where(allowed, scores, mask_fill)
    row_top = jnp.maximum(jnp.max(scores, axis=-1), sink_term)
    weights = jnp.where(allowed, jnp.exp(scores - row_top[..., None]), 0.0)
    row_total = jnp.sum(weights, axis=-1) + jnp.exp(sink_term - row_top)
    probs = (weights / row_total[..., None]).astype(jnp.bfloat16)
    block_out = jnp.einsum("hgqk,khd->qhgd", probs, near_values, preferred_element_type=jnp.float32)
    outputs = block_out.astype(jnp.bfloat16).reshape(query_span, kv_heads * group_size * HEAD_DIM)
    a_weight = a_out_w.reshape(local_heads, VALUE_DIM, a_out_w.shape[1])
    return lax.psum_scatter(
        (
            jnp.einsum("hqe,hen->qn", a_heads, a_weight, preferred_element_type=jnp.float32)
            + jnp.dot(outputs, b_out_w, preferred_element_type=jnp.float32)
        ).astype(jnp.bfloat16),
        "tp",
        scatter_dimension=0,
        tiled=True,
    )


def solution(mesh):
    return jax.shard_map(
        shards,
        mesh=mesh,
        in_specs=(
            P(("sp", "tp"), None),
            P(None, "tp"),
            P(None, "tp"),
            P(None, "tp"),
            P(None, "tp"),
            P(None, "tp"),
            P(None, "tp"),
            P("tp"),
            P(),
            P("tp"),
            P("tp", None),
            P("tp", None),
        ),
        out_specs=P(("sp", "tp"), None),
        check_vma=False,
    )
```

profile of v0, /device:TPU:0, one launch (start us, length us, event | category | flops | bytes accessed | tf_op | source)
XLA Modules:
  0.0 288.8 jit_solution(3257539258130049300)
XLA Ops:
  6.5 0.7 all-gather.3.cloned.1.call-update
  7.3 36.3 %all-gather.3.cloned.1.call-done = bf16[512,4096]{1,0:T(8,128)(2,1)} async-done(((bf16[64,4096]{1,0:T(8,128)(2,1)}), bf16[512,4096]{1,0:T(8,128)(2,1)}) %all-gather.3.cloned.1.call-update) | async-done | bytes 4194320 | tf_op jit(solution)/shard_map/all_gather | solution.py:120
  43.6 4.3 %convolution_convert_fusion.2 = bf16[512,256]{0,1:T(8,128)(2,1)S(1)} fusion(bf16[512,4096]{1,0:T(8,128)(2,1)} %all-gather.3.cloned.1.call-done, bf16[4096,256]{1,0:T(8,128)(2,1)} %param.19), kind=kOutput, calls=%fused_computation.37 | convolution fusion | flops 1073872896 | bytes 6553600 | tf_op jit(solution)/shard_map/dot_general | solution.py:112
  47.9 0.4 copy-done.9
  48.3 1.3 convolution_convert_fusion.3
  49.6 0.8 pad_maximum_fusion
  50.6 0.4 fusion.24
  51.0 3.8 %convolution_convert_fusion.4 = bf16[512,64]{0,1:T(8,128)(2,1)S(1)} fusion(bf16[512,4096]{1,0:T(8,128)(2,1)} %all-gather.3.cloned.1.call-done, bf16[4096,64]{0,1:T(8,128)(2,1)S(1)} %copy-done.4), kind=kOutput, calls=%fused_computation.39 | convolution fusion | flops 268468224 | bytes 4784128 | tf_op jit(solution)/shard_map/dot_general | solution.py:112
  54.9 1.4 convolution_convert_fusion.5
  56.3 3.5 %collective-permute-start = (bf16[128,128]{0,1:T(8,128)(2,1)S(1)}, bf16[128,128]{0,1:T(8,128)(2,1)S(1)}, u32[]{:S(2)}, u32[]{:S(2)}) collective-permute-start(bf16[128,128]{0,1:T(8,128)(2,1)S(1)} %pad_maximum_fusion.1), channel_id=1, source_target_pairs={{0,8},{8,16},{16,24},{24,32},{32,40},{40,48},{48,56},{56,64},{64,7... | collective-permute-start | bytes 98312 | tf_op jit(solution)/shard_map/ppermute | solution.py:18
  59.8 1.3 convolution_convert_fusion
  61.2 2.0 convolution_convert_fusion.1
  63.2 1.0 fusion.19
  64.3 0.1 broadcast_maximum_fusion
  64.3 1.3 fusion.20
  65.6 0.1 exponential_add_fusion
  65.7 1.8 fusion.25
  67.6 60.4 %all-gather.5.cloned.1.call-done = bf16[8192,512]{0,1:T(8,128)(2,1)} async-done(((bf16[512,512]{0,1:T(8,128)(2,1)}), bf16[8192,512]{0,1:T(8,128)(2,1)}) %all-gather.5.cloned.1.call-update) | async-done | bytes 8388624 | tf_op jit(solution)/shard_map/all_gather | solution.py:24
  128.0 5.9 %fusion.40 = (bf16[8192,256]{0,1:T(8,128)(2,1)}, bf16[8192,256]{0,1:T(8,128)(2,1)}) fusion(bf16[8192,512]{0,1:T(8,128)(2,1)} %all-gather.5.cloned.1.call-done), kind=kLoop, calls=%fused_computation.68 | loop fusion | bytes 16777216 | tf_op jit(solution)/shard_map/split | solution.py:25
  133.9 6.3 %copy.14 = bf16[8192,2,128]{2,0,1:T(8,128)(2,1)} copy(bf16[8192,2,128]{0,2,1:T(8,128)(2,1)} %bitcast.105) | data formatting | bytes 8388608 | tf_op jit(solution)/shard_map/while | solution.py:80
  140.3 31.0 %while.17 = (s32[]{:T(128)}, f32[2,2,512]{2,1,0:T(2,128)S(1)}, f32[2,2,512]{2,1,0:T(2,128)S(1)}, f32[2,2,512,128]{3,2,1,0:T(8,128)S(1)}, s32[512]{0:T(512)S(1)},...) while((s32[]{:T(128)}, f32[2,2,512]{2,1,0:T(2,128)S(1)}, ...), condition=%wide.region_5.6_spmd, body=%wide.region_0.5_spmd.sunk | while | flops 833623040 | bytes 30812476 | solution.py:80
  140.3 0.6 slice.65
  141.0 0.6 slice.64
  142.9 9.8 %conditional.2 = ((f32[2,2,512]{2,1,0:T(2,128)S(1)}, f32[2,2,512]{2,1,0:T(2,128)S(1)}, f32[2,2,512,128]{3,2,1,0:T(8,128)S(1)})) conditional(s32[]{:T(128)} %bitcast.103, (f32[2,2,512]{2,1,0:T(2,128)S(1)}, f32[2,2,512]{2,1,0:T(2,128)S(1)}, f32[2,2,512,128]{3,2,1,0:T(8,128)S(1)}) %tuple.51, (s32[512]{0:T(512)S(1)}, s32[1024]{0:T(1024)S(1)}, s32[]{:T(128)}, ...), branch_computations={%region_1.0_spmd, %region_2.4_spmd} | conditional | flops 833622016 | bytes 30808138 | solution.py:77
  143.0 0.4 broadcast_compare_fusion
  143.3 2.7 fusion
  146.1 2.1 fusion.2
  148.2 4.5 %fusion.6 = f32[2,2,512,128]{3,2,1,0:T(8,128)S(1)} fusion(f32[2,2,1024,512]{3,2,1,0:T(8,128)S(1)} %get-tuple-element.290, f32[2,2,512]{2,1,0:T(2,128)S(1)} %max.21, pred[512,1024]{0,1:T(8,128)(4,1)S(1)} %broadcast_compare_fusion, f32[2,2,512,128]{3,2,1,0:T(8,128)S(1)} %get-tuple-element.245, bf16[8192,2,128]{2,0,1:T(8,128)(2,1)} %get-tuple-element.246, ...), kind=kOutput, calls=%fused_computation.7 | convolution fusion | flops 547880960 | bytes 11550724 | tf_op jit(solution)/shard_map/while/body/eval_jaxpr/cond/branch_1_fun/hmqk,khe->hmqe/dot_general | solution.py:44
  152.7 0.6 slice.65
  153.4 0.6 slice.64
  155.4 0.6 slice.65
  156.0 0.6 slice.64
  158.1 0.6 slice.65
  158.7 0.6 slice.64
  160.7 0.6 slice.65
  161.4 0.6 slice.64
  163.4 0.6 slice.65
  164.0 0.6 slice.64
  166.0 0.6 slice.65
  166.7 0.6 slice.64
  168.7 0.6 slice.65
  169.3 0.6 slice.64
  171.3 0.3 broadcast_divide_fusion
  171.7 0.3 multiply_reduce_fusion
  172.0 1.3 fusion.30
  173.3 0.3 copy-done.3
  173.6 3.3 %fusion.18 = bf16[512,4096]{1,0:T(8,128)(2,1)} fusion(f32[512,4096,1]{1,0,2:T(8,128)S(1)} %fusion.30, bf16[512,256]{0,1:T(8,128)(2,1)S(1)} %bitcast.107, bf16[256,4096]{1,0:T(8,128)(2,1)S(1)} %copy-done.3), kind=kOutput, calls=%fused_computation.22 | convolution fusion | flops 1077936128 | bytes 14942208 | tf_op jit(solution)/shard_map/dot_general | solution.py:176
  176.9 105.4 %reduce-scatter.2.cloned.1.call-done = bf16[64,4096]{1,0:T(8,128)(2,1)} async-done(((bf16[512,4096]{1,0:T(8,128)(2,1)}), bf16[64,4096]{1,0:T(8,128)(2,1)}) %reduce-scatter.2.cloned.1.call-update) | async-done | bytes 524304 | tf_op jit(solution)/shard_map/reduce_scatter | solution.py:173
  (55 shorter events, 0.4 us)
Async XLA Ops:
  6.5 165.5 %copy-start = (bf16[256,4096]{1,0:T(8,128)(2,1)S(1)}, bf16[256,4096]{1,0:T(8,128)(2,1)}, u32[]{:S(2)}) copy-start(bf16[256,4096]{1,0:T(8,128)(2,1)} %param.26) | copy-start | bytes 6291460
  6.5 37.0 %all-gather.3.cloned.1.call-start = ((), (), s32[]{:S(2)}) async-start(), calls=%async_computation.1 | async-start | bytes 4718592 | tf_op jit(solution)/shard_map/all_gather | solution.py:120
  7.3 120.7 %all-gather.5.cloned.1.call-start = ((), (), s32[]{:S(2)}) async-start(), calls=%async_computation.2 | async-start | bytes 8912896 | tf_op jit(solution)/shard_map/all_gather | solution.py:24
  43.6 4.3 %copy-start.1 = (bf16[512,4096]{1,0:T(8,128)(2,1)S(1)}, bf16[512,4096]{1,0:T(8,128)(2,1)}, u32[]{:S(2)}) copy-start(bf16[512,4096]{1,0:T(8,128)(2,1)} %all-gather.3.cloned.1.call-done) | copy-start | bytes 12582916
  43.6 4.7 %copy-start.9 = (bf16[4096,256]{1,0:T(8,128)(2,1)S(1)}, bf16[4096,256]{1,0:T(8,128)(2,1)}, u32[]{:S(2)}) copy-start(bf16[4096,256]{1,0:T(8,128)(2,1)} %param.18) | copy-start | bytes 6291460
  48.3 2.7 copy-start.4
  49.6 5.2 %copy-start.5 = (bf16[4096,64]{0,1:T(8,128)(2,1)S(1)}, bf16[4096,64]{0,1:T(8,128)(2,1)}, u32[]{:S(2)}) copy-start(bf16[4096,64]{0,1:T(8,128)(2,1)} %param.21) | copy-start | bytes 1572868
  50.5 231.8 %reduce-scatter.2.cloned.1.call-start = ((), (), s32[]{:S(2)}) async-start(), calls=%async_computation.3 | async-start | bytes 4718592 | tf_op jit(solution)/shard_map/reduce_scatter | solution.py:173
  50.5 4.3 %copy-start.2 = (bf16[512,4096]{1,0:T(8,128)(2,1)S(1)}, bf16[512,4096]{1,0:T(8,128)(2,1)}, u32[]{:S(2)}) copy-start(bf16[512,4096]{1,0:T(8,128)(2,1)} %all-gather.3.cloned.1.call-done) | copy-start | bytes 12582916
  51.0 8.8 %copy-start.10 = (bf16[4096,256]{1,0:T(8,128)(2,1)S(1)}, bf16[4096,256]{1,0:T(8,128)(2,1)}, u32[]{:S(2)}) copy-start(bf16[4096,256]{1,0:T(8,128)(2,1)} %param.20) | copy-start | bytes 6291460
  56.3 4.9 %copy-start.11 = (bf16[4096,256]{1,0:T(8,128)(2,1)S(1)}, bf16[4096,256]{1,0:T(8,128)(2,1)}, u32[]{:S(2)}) copy-start(bf16[4096,256]{1,0:T(8,128)(2,1)} %param.17) | copy-start | bytes 6291460
  56.3 6.9 %collective-permute-start = (bf16[128,128]{0,1:T(8,128)(2,1)S(1)}, bf16[128,128]{0,1:T(8,128)(2,1)S(1)}, u32[]{:S(2)}, u32[]{:S(2)}) collective-permute-start(bf16[128,128]{0,1:T(8,128)(2,1)S(1)} %pad_maximum_fusion.1), channel_id=1, source_target_pairs={{0,8},{8,16},{16,24},{24,32},{32,40},{40,48},{48,56},{56,64},{64,7... | collective-permute-start | bytes 98312 | tf_op jit(solution)/shard_map/ppermute | solution.py:18
  63.2 1.1 copy-start.8
  140.3 31.4 %copy-start.6 = (f32[2]{0:T(128)S(1)}, f32[2]{0:T(128)}, u32[]{:S(2)}) copy-start(f32[2]{0:T(128)} %param.23) | copy-start | bytes 28
  140.3 31.7 %copy-start.7 = (f32[128]{0:T(128)S(1)}, f32[128]{0:T(128)}, u32[]{:S(2)}) copy-start(f32[128]{0:T(128)} %param.24) | copy-start | bytes 1540
  172.0 1.6 copy-start.3
Sparse Core Ops, SparseCore 0:
  9.0 34.4 all-gather.2
  50.6 77.3 all-gather.4
  177.0 105.1 reduce-scatter.1
where the time goes:
time: 290 us; the launch traced here: 289 us
  waiting for transfers between devices  203 us (70%)
  matrix products  28.8 us (10%)
  local copies, waits for them, and re-layouts  23 us (8%)
  between operations  13.4 us (5%)
  loops' own time  11.3 us (4%)
  other arithmetic  5.89 us (2%)
  starting transfers between devices  3.61 us (1%)
    reduce_scatter x1, waiting for transfers between devices, shards(): lax.psum_scatter((jnp.einsum('hqe,hen->qn', a_heads, a_weight, preferred_...  105 us
    all_gather x1, waiting for transfers between devices, side_by_side(): whole = lax.all_gather(both, axis, axis=dim, tiled=True)  60.4 us
    all_gather x1, waiting for transfers between devices, shards(): projected = project(lax.all_gather(inputs, 'tp', axis=0, tiled=True))  36.3 us
    dot_general x6, matrix products, project(): jnp.dot(shard_piece, matrix, preferred_element_type=jnp.float32)  14.1 us
    another operation x1, loops' own time, advance(): return lax.fori_loop(0, row_count // span_rows, one_span, states)  11.2 us
    while x1, local copies, waits for them, and re-layouts, advance(): return lax.fori_loop(0, row_count // span_rows, one_span, states)  6.32 us
    split x1, local copies, waits for them, and re-layouts, side_by_side(): jnp.split(whole, [sum(widths[:k]) for k in range(1, len(widths))], axis=a...  5.86 us
  transfers between devices with their start and end apart: 4, of which 3 were waited for; matrix products, arithmetic and copies ran while one was open for 5% of the time, Pallas kernels for 0%

commit v1 on v0

--- a/solution.py
+++ b/solution.py
@@ -10,6 +10,18 @@
 norm_eps = 0.0001
 head_scale = 0.8
 mask_fill = -1e30
+
+
+def doubled_up(x, axis, dim):
+    ways, here = (lax.axis_size(axis), lax.axis_index(axis))
+    grown, reach = (x, 1)
+    while reach < ways:
+        theirs = lax.ppermute(grown, axis, [(d, d ^ reach) for d in range(ways)])
+        mine_first = jnp.concatenate([grown, theirs], axis=dim)
+        theirs_first = jnp.concatenate([theirs, grown], axis=dim)
+        grown = jnp.where(here & reach == 0, mine_first, theirs_first)
+        reach = 2 * reach
+    return grown
 
 
 def from_behind(value, axis, by):
@@ -117,7 +129,7 @@
             axis=1,
         )
 
-    projected = project(lax.all_gather(inputs, "tp", axis=0, tiled=True))
+    projected = project(doubled_up(inputs, "tp", 0))
     seg_rows = projected.shape[0]
     column_edges = [0]
     for matrix in matrices:

time: 290 us -> 340 us (1.17)
  waiting for transfers between devices: 203 us -> 230 us
  matrix products: 28.8 us -> 42.9 us
  other arithmetic: 5.89 us -> 11.4 us
  starting transfers between devices: 3.61 us -> 8.77 us
    ppermute x0 -> x3, waiting for transfers between devices: none -> 71.5 us  [doubled_up(): theirs = lax.ppermute(grown, axis, [(d, d ^ reach) for d in range(ways)])]
    all_gather x1 -> x0, waiting for transfers between devices: 36.3 us -> none  [shards(): projected = project(lax.all_gather(inputs, 'tp', axis=0, tiled=True))]
    dot_general x6, matrix products: 14.1 us -> 28.2 us  [project(): jnp.dot(shard_piece, matrix, preferred_element_type=jnp.float32)]
    all_gather x1, waiting for transfers between devices: 60.4 us -> 52.9 us  [side_by_side(): whole = lax.all_gather(both, axis, axis=dim, tiled=True)]
    select_n x0 -> x2, other arithmetic: none -> 5.54 us  [doubled_up(): grown = jnp.where(here & reach == 0, mine_first, theirs_first)]
    ppermute x0 -> x3, starting transfers between devices: none -> 4.82 us  [doubled_up(): theirs = lax.ppermute(grown, axis, [(d, d ^ reach) for d in range(ways)])]
  transfers between devices with their start and end apart: 4 -> 6, of which waited for: 3 -> 5; matrix products, arithmetic and copies ran while one was open for 5% -> 7% of each run, Pallas kernels for 0% -> 0%
where the time goes in v1:
time: 340 us; the launch traced here: 339 us
  waiting for transfers between devices  230 us (68%)
  matrix products  42.9 us (13%)
  local copies, waits for them, and re-layouts  22 us (6%)
  between operations  13.7 us (4%)
  other arithmetic  11.4 us (3%)
  loops' own time  10.6 us (3%)
  starting transfers between devices  8.77 us (3%)
    reduce_scatter x1, waiting for transfers between devices, shards(): lax.psum_scatter((jnp.einsum('hqe,hen->qn', a_heads, a_weight, preferred_...  105 us
    ppermute x3, waiting for transfers between devices, doubled_up(): theirs = lax.ppermute(grown, axis, [(d, d ^ reach) for d in range(ways)])  71.5 us
    all_gather x1, waiting for transfers between devices, side_by_side(): whole = lax.all_gather(both, axis, axis=dim, tiled=True)  52.9 us
    dot_general x6, matrix products, project(): jnp.dot(shard_piece, matrix, preferred_element_type=jnp.float32)  28.2 us
    another operation x1, loops' own time, advance(): return lax.fori_loop(0, row_count // span_rows, one_span, states)  10.5 us
  transfers between devices with their start and end apart: 6, of which 5 were waited for; matrix products, arithmetic and copies ran while one was open for 7% of the time, Pallas kernels for 0%

profile of v1, /device:TPU:0, one launch (start us, length us, event | category | flops | bytes accessed | tf_op | source)
XLA Modules:
  0.0 339.1 jit_solution(6440196751606363492)
XLA Ops:
  6.5 2.2 collective-permute-done
  8.8 1.9 maximum_select_fusion.2
  10.7 1.7 collective-permute-start.1
  12.4 23.7 %collective-permute-done.1 = bf16[128,4096]{1,0:T(8,128)(2,1)} collective-permute-done((bf16[128,4096]{1,0:T(8,128)(2,1)S(1)}, bf16[128,4096]{1,0:T(8,128)(2,1)}, u32[]{:S(2)}, u32[]{:S(2)}) %collective-permute-start.1) | collective-permute-done | bytes 1048608 | tf_op jit(solution)/shard_map/ppermute | solution.py:19
  36.1 3.6 %maximum_select_fusion.1 = bf16[256,4096]{1,0:T(8,128)(2,1)} fusion(bf16[128,4096]{1,0:T(8,128)(2,1)} %collective-permute-done.1, bf16[128,4096]{1,0:T(8,128)(2,1)S(1)} %maximum_select_fusion.2, pred[]{:T(512)S(6)} %eq.10), kind=kLoop, calls=%fused_computation.31 | loop fusion | flops 9437184 | bytes 4194305 | tf_op jit(solution)/shard_map/jit(_where)/select_n | solution.py:22
  39.7 3.1 collective-permute-start.2
  42.9 45.5 %collective-permute-done.2 = bf16[256,4096]{1,0:T(8,128)(2,1)} collective-permute-done((bf16[256,4096]{1,0:T(8,128)(2,1)}, bf16[256,4096]{1,0:T(8,128)(2,1)}, u32[]{:S(2)}, u32[]{:S(2)}) %collective-permute-start.2) | collective-permute-done | bytes 2097184 | tf_op jit(solution)/shard_map/ppermute | solution.py:19
  88.4 5.5 %convolution_convert_fusion.2 = bf16[512,256]{0,1:T(8,128)(2,1)S(1)} fusion(bf16[4096,256]{1,0:T(8,128)(2,1)} %param.19, bf16[256,4096]{1,0:T(8,128)(2,1)} %collective-permute-done.2, bf16[256,4096]{1,0:T(8,128)(2,1)} %maximum_select_fusion.1, pred[]{:T(512)S(6)} %eq.9), kind=kOutput, calls=%fused_computation.39 | convolution fusion | flops 1092747264 | bytes 6553601 | tf_op jit(solution)/shard_map/dot_general | solution.py:124
  93.9 4.4 %convolution_convert_fusion.3 = bf16[512,256]{0,1:T(8,128)(2,1)S(1)} fusion(bf16[4096,256]{1,0:T(8,128)(2,1)S(1)} %copy-done.5, bf16[256,4096]{1,0:T(8,128)(2,1)} %collective-permute-done.2, bf16[256,4096]{1,0:T(8,128)(2,1)} %maximum_select_fusion.1, pred[]{:T(512)S(6)} %eq.9), kind=kOutput, calls=%fused_computation.40 | convolution fusion | flops 1092747264 | bytes 6553601 | tf_op jit(solution)/shard_map/dot_general | solution.py:124
  98.4 0.8 pad_maximum_fusion
  99.3 0.4 fusion.24
  99.8 4.3 %convolution_convert_fusion.5 = bf16[512,64]{0,1:T(8,128)(2,1)S(1)} fusion(bf16[4096,64]{0,1:T(8,128)(2,1)S(1)} %copy-done.8, bf16[256,4096]{1,0:T(8,128)(2,1)} %collective-permute-done.2, bf16[256,4096]{1,0:T(8,128)(2,1)} %maximum_select_fusion.1, pred[]{:T(512)S(6)} %eq.9), kind=kOutput, calls=%fused_computation.42 | convolution fusion | flops 287342592 | bytes 4784129 | tf_op jit(solution)/shard_map/dot_general | solution.py:124
  104.1 4.3 %convolution_convert_fusion.4 = bf16[512,64]{0,1:T(8,128)(2,1)S(1)} fusion(bf16[4096,64]{0,1:T(8,128)(2,1)S(1)} %copy-done.9, bf16[256,4096]{1,0:T(8,128)(2,1)} %collective-permute-done.2, bf16[256,4096]{1,0:T(8,128)(2,1)} %maximum_select_fusion.1, pred[]{:T(512)S(6)} %eq.9), kind=kOutput, calls=%fused_computation.41 | convolution fusion | flops 287342592 | bytes 4784129 | tf_op jit(solution)/shard_map/dot_general | solution.py:124
  108.5 3.9 %collective-permute-start.3 = (bf16[128,128]{0,1:T(8,128)(2,1)S(1)}, bf16[128,128]{0,1:T(8,128)(2,1)S(1)}, u32[]{:S(2)}, u32[]{:S(2)}) collective-permute-start(bf16[128,128]{0,1:T(8,128)(2,1)S(1)} %pad_maximum_fusion.1), channel_id=1, source_target_pairs={{0,8},{8,16},{16,24},{24,32},{32,40},{40,48},{48,56},{56,64},{64,7... | collective-permute-start | bytes 98312 | tf_op jit(solution)/shard_map/ppermute | solution.py:30
  112.4 5.2 %convolution_convert_fusion.1 = bf16[512,256]{0,1:T(8,128)(2,1)} fusion(bf16[4096,256]{1,0:T(8,128)(2,1)S(1)} %copy-done.6, bf16[256,4096]{1,0:T(8,128)(2,1)} %collective-permute-done.2, bf16[256,4096]{1,0:T(8,128)(2,1)} %maximum_select_fusion.1, pred[]{:T(512)S(6)} %eq.9), kind=kOutput, calls=%fused_computation.38 | convolution fusion | flops 1092747264 | bytes 6553601 | tf_op jit(solution)/shard_map/dot_general | solution.py:124
  117.6 4.4 %convolution_convert_fusion = bf16[512,256]{0,1:T(8,128)(2,1)S(1)} fusion(bf16[4096,256]{1,0:T(8,128)(2,1)S(1)} %copy-done.7, bf16[256,4096]{1,0:T(8,128)(2,1)} %collective-permute-done.2, bf16[256,4096]{1,0:T(8,128)(2,1)} %maximum_select_fusion.1, pred[]{:T(512)S(6)} %eq.9), kind=kOutput, calls=%fused_computation.37 | convolution fusion | flops 1092747264 | bytes 6553601 | tf_op jit(solution)/shard_map/dot_general | solution.py:124
  122.0 1.1 fusion.19
  123.2 1.3 fusion.20
  124.6 1.8 fusion.25
  126.4 52.9 %all-gather.2.cloned.1.call-done = bf16[8192,512]{0,1:T(8,128)(2,1)} async-done(((bf16[512,512]{0,1:T(8,128)(2,1)}), bf16[8192,512]{0,1:T(8,128)(2,1)}) %all-gather.2.cloned.1.call-update) | async-done | bytes 8388624 | tf_op jit(solution)/shard_map/all_gather | solution.py:36
  179.3 5.9 %fusion.40 = (bf16[8192,256]{0,1:T(8,128)(2,1)}, bf16[8192,256]{0,1:T(8,128)(2,1)}) fusion(bf16[8192,512]{0,1:T(8,128)(2,1)} %all-gather.2.cloned.1.call-done), kind=kLoop, calls=%fused_computation.71 | loop fusion | bytes 16777216 | tf_op jit(solution)/shard_map/split | solution.py:37
  185.2 6.3 %copy.14 = bf16[8192,2,128]{2,0,1:T(8,128)(2,1)} copy(bf16[8192,2,128]{0,2,1:T(8,128)(2,1)} %bitcast.99) | data formatting | bytes 8388608 | tf_op jit(solution)/shard_map/while | solution.py:92
  191.6 29.7 %while.17 = (s32[]{:T(128)}, f32[2,2,512]{2,1,0:T(2,128)S(1)}, f32[2,2,512]{2,1,0:T(2,128)S(1)}, f32[2,2,512,128]{3,2,1,0:T(8,128)S(1)}, s32[512]{0:T(512)S(1)},...) while((s32[]{:T(128)}, f32[2,2,512]{2,1,0:T(2,128)S(1)}, ...), condition=%wide.region_5.6_spmd, body=%wide.region_0.5_spmd.sunk | while | flops 833623040 | bytes 30812476 | solution.py:92
  191.9 0.6 slice.65
  192.4 0.6 slice.64
  194.3 9.8 %conditional.2 = ((f32[2,2,512]{2,1,0:T(2,128)S(1)}, f32[2,2,512]{2,1,0:T(2,128)S(1)}, f32[2,2,512,128]{3,2,1,0:T(8,128)S(1)})) conditional(s32[]{:T(128)} %bitcast.97, (f32[2,2,512]{2,1,0:T(2,128)S(1)}, f32[2,2,512]{2,1,0:T(2,128)S(1)}, f32[2,2,512,128]{3,2,1,0:T(8,128)S(1)}) %tuple.51, (s32[512]{0:T(512)S(1)}, s32[1024]{0:T(1024)S(1)}, s32[]{:T(128)}, ...), branch_computations={%region_1.1_spmd, %region_2.4_spmd} | conditional | flops 833622016 | bytes 30808138 | solution.py:89
  194.3 0.4 broadcast_compare_fusion
  194.7 2.7 fusion
  197.4 2.1 fusion.2
  199.6 4.5 %fusion.6 = f32[2,2,512,128]{3,2,1,0:T(8,128)S(1)} fusion(f32[2,2,1024,512]{3,2,1,0:T(8,128)S(1)} %get-tuple-element.290, f32[2,2,512]{2,1,0:T(2,128)S(1)} %max.21, pred[512,1024]{0,1:T(8,128)(4,1)S(1)} %broadcast_compare_fusion, f32[2,2,512,128]{3,2,1,0:T(8,128)S(1)} %get-tuple-element.245, bf16[8192,2,128]{2,0,1:T(8,128)(2,1)} %get-tuple-element.246, ...), kind=kOutput, calls=%fused_computation.7 | convolution fusion | flops 547880960 | bytes 11550724 | tf_op jit(solution)/shard_map/while/body/eval_jaxpr/cond/branch_1_fun/hmqk,khe->hmqe/dot_general | solution.py:56
  204.1 0.6 slice.65
  204.7 0.6 slice.64
  206.5 0.6 slice.65
  207.1 0.6 slice.64
  209.0 0.6 slice.65
  209.6 0.6 slice.64
  211.5 0.6 slice.65
  212.1 0.6 slice.64
  213.9 0.6 slice.65
  214.5 0.6 slice.64
  216.4 0.6 slice.65
  217.0 0.6 slice.64
  218.9 0.6 slice.65
  219.5 0.6 slice.64
  221.3 0.3 broadcast_divide_fusion
  222.0 1.3 fusion.30
  223.6 3.3 fusion.18
  226.9 105.3 %reduce-scatter.2.cloned.1.call-done = bf16[64,4096]{1,0:T(8,128)(2,1)} async-done(((bf16[512,4096]{1,0:T(8,128)(2,1)}), bf16[64,4096]{1,0:T(8,128)(2,1)}) %reduce-scatter.2.cloned.1.call-update) | async-done | bytes 524304 | tf_op jit(solution)/shard_map/reduce_scatter | solution.py:185
  (56 shorter events, 1.1 us)
Async XLA Ops:
  6.5 215.4 %copy-start = (bf16[256,4096]{1,0:T(8,128)(2,1)S(1)}, bf16[256,4096]{1,0:T(8,128)(2,1)}, u32[]{:S(2)}) copy-start(bf16[256,4096]{1,0:T(8,128)(2,1)} %param.26) | copy-start | bytes 6291460
  6.5 172.8 %all-gather.2.cloned.1.call-start = ((), (), s32[]{:S(2)}) async-start(), calls=%async_computation.1 | async-start | bytes 8912896 | tf_op jit(solution)/shard_map/all_gather | solution.py:36
  6.5 2.3 collective-permute-start
  10.7 25.4 %collective-permute-start.1 = (bf16[128,4096]{1,0:T(8,128)(2,1)S(1)}, bf16[128,4096]{1,0:T(8,128)(2,1)}, u32[]{:S(2)}, u32[]{:S(2)}) collective-permute-start(bf16[128,4096]{1,0:T(8,128)(2,1)S(1)} %maximum_select_fusion.2), channel_id=1, source_target_pairs={{0,2},{1,3},{2,0},{3,1},{4,6},{5,7},{6,4},{7,5},{8,10},{9,11},{10,... | collective-permute-start | bytes 3145736 | tf_op jit(solution)/shard_map/ppermute | solution.py:19
  39.7 48.6 %collective-permute-start.2 = (bf16[256,4096]{1,0:T(8,128)(2,1)}, bf16[256,4096]{1,0:T(8,128)(2,1)}, u32[]{:S(2)}, u32[]{:S(2)}) collective-permute-start(bf16[256,4096]{1,0:T(8,128)(2,1)} %maximum_select_fusion.1), channel_id=1, source_target_pairs={{0,4},{1,5},{2,6},{3,7},{4,0},{5,1},{6,2},{7,3},{8,12},{9,13},{10,... | collective-permute-start | bytes 6291464 | tf_op jit(solution)/shard_map/ppermute | solution.py:19
  42.9 51.0 %copy-start.5 = (bf16[4096,256]{1,0:T(8,128)(2,1)S(1)}, bf16[4096,256]{1,0:T(8,128)(2,1)}, u32[]{:S(2)}) copy-start(bf16[4096,256]{1,0:T(8,128)(2,1)} %param.18) | copy-start | bytes 6291460
  93.9 5.8 %copy-start.8 = (bf16[4096,64]{0,1:T(8,128)(2,1)S(1)}, bf16[4096,64]{0,1:T(8,128)(2,1)}, u32[]{:S(2)}) copy-start(bf16[4096,64]{0,1:T(8,128)(2,1)} %param.21) | copy-start | bytes 1572868
  99.2 233.0 %reduce-scatter.2.cloned.1.call-start = ((), (), s32[]{:S(2)}) async-start(), calls=%async_computation.2 | async-start | bytes 4718592 | tf_op jit(solution)/shard_map/reduce_scatter | solution.py:185
  99.8 4.3 %copy-start.9 = (bf16[4096,64]{0,1:T(8,128)(2,1)S(1)}, bf16[4096,64]{0,1:T(8,128)(2,1)}, u32[]{:S(2)}) copy-start(bf16[4096,64]{0,1:T(8,128)(2,1)} %param.22) | copy-start | bytes 1572868
  104.1 8.3 %copy-start.6 = (bf16[4096,256]{1,0:T(8,128)(2,1)S(1)}, bf16[4096,256]{1,0:T(8,128)(2,1)}, u32[]{:S(2)}) copy-start(bf16[4096,256]{1,0:T(8,128)(2,1)} %param.17) | copy-start | bytes 6291460
  108.4 9.1 %copy-start.7 = (bf16[4096,256]{1,0:T(8,128)(2,1)S(1)}, bf16[4096,256]{1,0:T(8,128)(2,1)}, u32[]{:S(2)}) copy-start(bf16[4096,256]{1,0:T(8,128)(2,1)} %param.20) | copy-start | bytes 6291460
  108.5 13.5 %collective-permute-start.3 = (bf16[128,128]{0,1:T(8,128)(2,1)S(1)}, bf16[128,128]{0,1:T(8,128)(2,1)S(1)}, u32[]{:S(2)}, u32[]{:S(2)}) collective-permute-start(bf16[128,128]{0,1:T(8,128)(2,1)S(1)} %pad_maximum_fusion.1), channel_id=1, source_target_pairs={{0,8},{8,16},{16,24},{24,32},{32,40},{40,48},{48,56},{56,64},{64,7... | collective-permute-start | bytes 98312 | tf_op jit(solution)/shard_map/ppermute | solution.py:30
  122.0 1.1 copy-start.4
  191.6 30.1 %copy-start.2 = (f32[2]{0:T(128)S(1)}, f32[2]{0:T(128)}, u32[]{:S(2)}) copy-start(f32[2]{0:T(128)} %param.23) | copy-start | bytes 28
  191.6 30.4 %copy-start.3 = (f32[128]{0:T(128)S(1)}, f32[128]{0:T(128)}, u32[]{:S(2)}) copy-start(f32[128]{0:T(128)} %param.24) | copy-start | bytes 1540
  222.0 1.6 copy-start.1
Sparse Core Ops, SparseCore 0:
  99.3 79.9 all-gather.1
  227.0 105.1 reduce-scatter.1
